TPU v7x, 32 devices: a whole 2x2x4 slice. The times are simulated.
32 devices in a mesh: ep: 8 (over z, x), tp: 4 (over y, core).
Axes of the slice: x: 2, y: 2, z: 4, core: 2. Of those that a mesh axis runs over, the one named last changes fastest.
Arguments:
- queries: bfloat16 [8192, 2048], P('ep', 'tp'), may hold values from -6 to 6
- key_vectors: bfloat16 [8192, 2048], P('ep', 'tp'), may hold values from -6 to 6
- value_vectors: bfloat16 [8192, 4096], P('ep', 'tp'), may hold values from -6 to 6
- decay_logit: float32 [8192, 2048], P('ep', 'tp'), may hold values from -11 to 16
- head_gain: float32 [256], replicated, may hold values from 0.1 to 1.9
- routed_rows: bfloat16 [2048, 4096], P('ep'), may hold values from -6 to 6
- pre_gain: float32 [4096], replicated, may hold values from 0.1 to 1.9
- expert_pick: int32 [2048, 2], P('ep'), may hold values from 0 to 7, as said below
- route_weight: float32 [2048, 2], P('ep'), may hold values from 0.2 to 1
- gate_weight: bfloat16 [8, 4096, 2048], P('ep', None, 'tp'), may hold values from -0.09375 to 0.09375
- up_weight: bfloat16 [8, 4096, 2048], P('ep', None, 'tp'), may hold values from -0.09375 to 0.09375
- down_weight: bfloat16 [8, 2048, 4096], P('ep', 'tp'), may hold values from -0.125 to 0.125
- post_gain: float32 [4096], replicated, may hold values from 0.1 to 1.9
Outputs:
- mixed_heads: bfloat16 [8192, 4096], P('ep', 'tp')
- routed_out: bfloat16 [2048, 4096], P(('ep', 'tp'))
Inputs may be any that keep to these rules, and one draw needn't show every extreme that they name: `expert_pick`: each row names 2 different experts, both in the same one of 4 equal groups of consecutive expert numbers. In every aligned block of 64 rows no expert is named more than 32 times, and some expert exactly 32 times.
All inputs are finite; a program needn't handle non-finite values.
Results may differ from a plain program's by a relative error of at most 0.015.
Values may be sent and summed in bfloat16 or wider, within the bound.
A program may use at most 128 MiB of HBM per device.

v0:
```python
import jax
import jax.numpy as jnp
from jax import lax
from jax.sharding import PartitionSpec as P

DK = 128
DV = 256
BLK = 64


def entering(x, axis, join, neutral):
    place = lax.axis_index(axis)
    gathered = jax.tree.map(
        lambda a, kind: lax.all_gather(a.astype(kind), axis), x, (jnp.bfloat16, jnp.bfloat16)
    )
    state = jax.tree.map(lambda a, e: jnp.zeros_like(a) + jnp.asarray(e, a.dtype), x, neutral)

    def one(lap, state):
        return join(
            state,
            jax.tree.map(
                lambda a, own: lax.dynamic_index_in_dim(a, lap, 0, False).astype(own.dtype),
                gathered,
                x,
            ),
        )

    return lax.fori_loop(0, place, one, state)


def chain_join(earlier, later_part):
    decay_first, initial_memory_matrix = earlier
    decay_second, state_second = later_part
    return (
        decay_first * decay_second,
        initial_memory_matrix * decay_second[..., None] + state_second,
    )


def row_norm(values, gain):
    return values * lax.rsqrt(jnp.mean(values * values, axis=-1, keepdims=True) + 1e-06) * gain


def token_mixer(queries, key_vectors, value_vectors, decay_logit, head_gain):
    blocks = queries.shape[0] // BLK
    heads_here = queries.shape[1] // DK
    key_shape = (blocks, BLK, heads_here, DK)
    log_rate = jax.nn.log_sigmoid(decay_logit).reshape(key_shape) / 16.0
    cumulative = jnp.cumsum(log_rate, axis=1)
    ending = cumulative[:, -1]
    query_rows = queries.reshape(key_shape)
    key_rows = key_vectors.reshape(key_shape)
    value_rows = value_vectors.reshape(blocks, BLK, heads_here, DV)
    query_decay = (query_rows * jnp.exp(cumulative)).astype(jnp.bfloat16)
    key_decay = (key_rows * jnp.exp(-cumulative)).astype(jnp.bfloat16)
    key_to_end = (key_rows * jnp.exp(ending[:, None] - cumulative)).astype(jnp.bfloat16)
    update = jnp.einsum(
        "njhd,njhe->nhde", key_to_end, value_rows, preferred_element_type=jnp.float32
    )
    step_decay = jnp.exp(ending)

    def advance(carry, inputs):
        carry_state, carry_decay = carry
        block_update, block_decay = inputs
        next_carry = (
            carry_state * block_decay[..., None] + block_update,
            carry_decay * block_decay,
        )
        return (next_carry, (carry_state, carry_decay))

    start_carry = (jnp.zeros_like(update[0]), jnp.ones_like(step_decay[0]))
    (final_state, total_decay), (local_states, local_decay) = lax.scan(
        advance, start_carry, (update, step_decay)
    )
    incoming = entering(
        (total_decay, final_state),
        "ep",
        chain_join,
        (jnp.ones_like(total_decay), jnp.zeros_like(final_state)),
    )
    causal_mask = jnp.tril(jnp.ones((BLK, BLK), dtype=bool))
    scores = jnp.einsum(
        "nihd,njhd->nhij", query_decay, key_decay, preferred_element_type=jnp.float32
    )
    weights = jnp.where(causal_mask, scores, 0.0).astype(jnp.bfloat16)
    inside = jnp.einsum("nhij,njhe->nihe", weights, value_rows, preferred_element_type=jnp.float32)
    states = (local_states + incoming[1][None] * local_decay[..., None]).astype(jnp.bfloat16)
    carried = jnp.einsum("nihd,nhde->nihe", query_decay, states, preferred_element_type=jnp.float32)
    outputs = row_norm(inside + carried, head_gain).astype(jnp.bfloat16)
    return outputs.reshape(queries.shape[0], heads_here * DV)


def routed_experts(
    routed_rows, pre_gain, expert_pick, route_weight, gate_weight, up_weight, down_weight, post_gain
):
    tp_count = lax.axis_size("tp")
    ep_count = lax.axis_size("ep")
    part_index = lax.axis_index("tp")
    ep_rows, model_width = routed_rows.shape
    part_rows = ep_rows // tp_count
    top_count = expert_pick.shape[1]
    experts = ep_count * gate_weight.shape[0]
    capacity = 2 * top_count * part_rows // experts
    normed = row_norm(routed_rows.astype(jnp.float32), pre_gain).astype(jnp.bfloat16)
    padded = jnp.concatenate([normed, jnp.zeros((1, model_width), jnp.bfloat16)], axis=0)
    picks = expert_pick.reshape(tp_count, part_rows * top_count)
    matches = (picks[:, :, None] == jnp.arange(experts, dtype=jnp.int32)[None, None, :]).astype(
        jnp.int32
    )
    slots = jnp.sum((jnp.cumsum(matches, axis=1) - 1) * matches, axis=2)
    targets = picks * capacity + slots
    sources = (
        jnp.arange(part_rows * top_count, dtype=jnp.int32)[None, :] // top_count
        + part_rows * jnp.arange(tp_count, dtype=jnp.int32)[:, None]
    )
    slice_offset_index = jnp.broadcast_to(
        jnp.arange(tp_count, dtype=jnp.int32)[:, None], targets.shape
    )
    table = (
        jnp.full((tp_count, experts * capacity), ep_rows, jnp.int32)
        .at[slice_offset_index, targets]
        .set(sources)
    )
    gate_local = gate_weight[0]
    up_local = up_weight[0]
    down_local = down_weight[0]
    own_table = lax.dynamic_slice_in_dim(table, part_index, 1, 0)
    outgoing = padded[own_table].reshape(1, ep_count, capacity, model_width)
    arrived = lax.all_gather(
        lax.all_to_all(outgoing, "ep", split_axis=1, concat_axis=1, tiled=True),
        "tp",
        axis=0,
        tiled=True,
    )
    gate_act = jnp.einsum("pskd,df->pskf", arrived, gate_local, preferred_element_type=jnp.float32)
    up_act = jnp.einsum("pskd,df->pskf", arrived, up_local, preferred_element_type=jnp.float32)
    hidden = (jax.nn.silu(gate_act) * up_act).astype(jnp.bfloat16)
    summed = lax.psum_scatter(
        jnp.einsum("pskf,fd->pskd", hidden, down_local, preferred_element_type=jnp.float32).astype(
            jnp.bfloat16
        ),
        "tp",
        scatter_dimension=0,
        tiled=True,
    )
    returned = lax.all_to_all(summed, "ep", split_axis=1, concat_axis=1, tiled=True)
    flattened = returned.reshape(experts * capacity, model_width)
    my_slots = lax.dynamic_slice_in_dim(targets, part_index, 1, 0).reshape(part_rows, top_count)
    my_weight = lax.dynamic_slice_in_dim(route_weight, part_index * part_rows, part_rows, 0)
    combined = jnp.sum(flattened[my_slots].astype(jnp.float32) * my_weight[:, :, None], axis=1)
    return row_norm(combined, post_gain).astype(jnp.bfloat16)


def on_device(
    queries,
    key_vectors,
    value_vectors,
    decay_logit,
    head_gain,
    routed_rows,
    pre_gain,
    expert_pick,
    route_weight,
    gate_weight,
    up_weight,
    down_weight,
    post_gain,
):
    mixed_heads = token_mixer(queries, key_vectors, value_vectors, decay_logit, head_gain)
    routed_out = routed_experts(
        routed_rows,
        pre_gain,
        expert_pick,
        route_weight,
        gate_weight,
        up_weight,
        down_weight,
        post_gain,
    )
    return (mixed_heads, routed_out)


def solution(mesh):
    placed = (
        P("ep", "tp"),
        P("ep", "tp"),
        P("ep", "tp"),
        P("ep", "tp"),
        P(),
        P("ep", None),
        P(),
        P("ep", None),
        P("ep", None),
        P("ep", None, "tp"),
        P("ep", None, "tp"),
        P("ep", "tp", None),
        P(),
    )
    return jax.shard_map(
        on_device,
        mesh=mesh,
        in_specs=placed,
        out_specs=(P("ep", "tp"), P(("ep", "tp"), None)),
        check_vma=False,
    )
```

profile of v0, /device:TPU:24, one launch (start us, length us, event | category | flops | bytes accessed | tf_op | source)
XLA Modules:
  0.0 356.1 jit_solution(9693365549622294666)
XLA Ops:
  9.6 2.1 fusion
  12.9 24.7 %scatter_fusion = s32[4,256]{1,0:T(4,128)S(1)} fusion(s32[4,256]{1,0:T(4,128)S(1)} %broadcast_in_dim.35, s32[512]{0:T(512)S(1)} %fusion.36, s32[512]{0:T(512)S(1)} %add_bitcast_fusion), kind=kCustom, calls=%fused_computation.2 | custom fusion | bytes 10240 | tf_op jit(solution)/shard_map/scatter | solution.py:122
  38.5 3.2 gather_fusion
  41.7 51.7 %all_to_all.10 = bf16[1,8,32,4096]{3,2,0,1:T(8,128)(2,1)} all-to-all(bf16[1,8,32,4096]{3,2,0,1:T(8,128)(2,1)} %bitcast.88), channel_id=1, replica_groups=mesh['ep'=8,'tp'=4] {'ep'}, dimensions={1} | all-to-all | bytes 4194304 | tf_op jit(solution)/shard_map/all_to_all | solution.py:130
  93.5 2.8 fusion.12
  96.3 1.9 div.38
  98.2 3.4 reshape.181
  101.6 3.4 reshape.189
  105.0 2.8 reshape.188
  107.8 1.9 fusion.14
  110.7 4.3 %multiply_convert_fusion.3 = (bf16[16,64,4,128]{3,0,1,2:T(8,128)(2,1)}, bf16[16,64,4,128]{3,0,1,2:T(8,128)(2,1)S(1)}, bf16[16,64,4,128]{3,0,1,2:T(8,128)(2,1)}) fusion(f32[16,64,4,128]{3,0,1,2:T(8,128)S(1)} %fusion.14, f32[16,64,4,128]{3,2,1,0:T(4,128)S(1)} %copy-done.3, f32[16,4,128]{2,0,1:T(8,128)S(1)} %slice_bitcast_fusion, ...), kind=kLoop, calls=%fused_computation.39 | loop fusion | flops 4194304 | bytes 9469952 | tf_op jit(solution)/shard_map/convert_element_type | solution.py:55
  115.0 4.5 %fusion.20 = f32[16,4,128,256]{3,2,1,0:T(8,128)} fusion(bf16[16,64,4,256]{3,2,1,0:T(4,128)(2,1)S(1)} %reshape.181, bf16[16,64,4,128]{3,0,1,2:T(8,128)(2,1)S(1)} %get-tuple-element.161), kind=kOutput, calls=%fused_computation.40 | convolution fusion | flops 268435456 | bytes 11534336 | tf_op jit(solution)/shard_map/njhd,njhe->nhde/dot_general | solution.py:57
  119.5 33.5 %all-gather.6.cloned.1.call-done = bf16[4,8,32,4096]{3,2,1,0:T(8,128)(2,1)} async-done(((bf16[1,8,32,4096]{3,2,1,0:T(8,128)(2,1)}), bf16[4,8,32,4096]{3,2,1,0:T(8,128)(2,1)}) %all-gather.6.cloned.1.call-update) | async-done | bytes 8388624 | tf_op jit(solution)/shard_map/all_gather | solution.py:129
  153.0 8.1 %fusion.5 = f32[4,8,32,512]{3,2,1,0:T(8,128)S(1)} fusion(bf16[4,8,32,4096]{3,2,1,0:T(8,128)(2,1)} %all-gather.6.cloned.1.call-done, bf16[1,4096,512]{2,1,0:T(8,128)(2,1)} %param.27), kind=kOutput, calls=%fused_computation.20 | convolution fusion | flops 4294967296 | bytes 14680064 | tf_op jit(solution)/shard_map/pskd,df->pskf/dot_general | solution.py:136
  161.2 16.0 %convolution_convert_fusion = bf16[4,8,32,4096]{3,2,1,0:T(8,128)(2,1)} fusion(bf16[1,512,4096]{2,1,0:T(8,128)(2,1)} %param.28, f32[4,8,32,512]{3,2,1,0:T(8,128)S(1)} %fusion.5, bf16[4,8,32,4096]{3,2,1,0:T(8,128)(2,1)} %all-gather.6.cloned.1.call-done, bf16[1,4096,512]{2,1,0:T(8,128)(2,1)} %param.26), kind=kOutput, calls=%fused_computation.11 | convolution fusion | flops 8597274624 | bytes 27262976 | tf_op jit(solution)/shard_map/pskf,fd->pskd/dot_general | solution.py:139
  177.3 34.7 %while.30 = (s32[]{:T(128)}, f32[4,128,256]{2,1,0:T(8,128)S(1)}, f32[4,128]{1,0:T(4,128)S(1)}, f32[16,4,128,256]{3,2,1,0:T(8,128)}, f32[16,4,128]{2,1,0:T(4,128)...) while((s32[]{:T(128)}, f32[4,128,256]{2,1,0:T(8,128)S(1)}, ...), condition=%wide.region_2.3_spmd.clone, body=%wide.region_1.2_spmd.clone.sunk | while | flops 525827 | bytes 2637954 | solution.py:72
  178.1 1.2 bitcast_add_fusion.4
  180.2 1.2 bitcast_add_fusion.4
  182.4 1.4 bitcast_add_fusion.4
  184.7 1.3 bitcast_add_fusion.4
  186.9 1.4 bitcast_add_fusion.4
  189.2 1.4 bitcast_add_fusion.4
  191.4 1.2 bitcast_add_fusion.4
  193.6 1.2 bitcast_add_fusion.4
  195.7 1.2 bitcast_add_fusion.4
  197.8 1.2 bitcast_add_fusion.4
  200.0 1.4 bitcast_add_fusion.4
  202.2 1.2 bitcast_add_fusion.4
  204.4 1.2 bitcast_add_fusion.4
  206.5 1.2 bitcast_add_fusion.4
  208.6 1.2 bitcast_add_fusion.4
  210.7 1.2 bitcast_add_fusion.4
  212.9 35.9 %reduce-scatter.2.cloned.1.call-done = bf16[1,8,32,4096]{3,2,1,0:T(8,128)(2,1)} async-done(((bf16[4,8,32,4096]{3,2,1,0:T(8,128)(2,1)}), bf16[1,8,32,4096]{3,2,1,0:T(8,128)(2,1)}) %reduce-scatter.2.cloned.1.call-update) | async-done | bytes 2097168 | tf_op jit(solution)/shard_map/reduce_scatter | solution.py:138
  248.8 6.0 %all-to-all-start.1 = ((bf16[1,8,32,4096]{3,2,0,1:T(8,128)(2,1)}), bf16[1,8,32,4096]{3,2,0,1:T(8,128)(2,1)S(1)}, u32[]{:S(2)}, u32[]{:S(2)}) async-start(bf16[1,8,32,4096]{3,2,0,1:T(8,128)(2,1)} %bitcast.91), calls=%async_computation.2 | async-start | bytes 4194304 | tf_op jit(solution)/shard_map/all_to_all | solution.py:146
  255.1 58.9 %all-gather.2 = bf16[8,4,128]{2,1,0:T(4,128)(2,1)S(1)} all-gather(bf16[1,4,128]{2,1,0:T(4,128)(2,1)S(1)} %convert_bitcast_fusion), channel_id=2, replica_groups=mesh['ep'=8,'tp'=4] {'ep'}, dimensions={0}, use_global_device_ids=true | all-gather | bytes 9216 | tf_op jit(solution)/shard_map/all_gather | solution.py:14
  314.1 7.1 %while.29 = (s32[]{:T(128)}, f32[4,128,256]{2,1,0:T(8,128)S(1)}, s32[]{:T(128)}, bf16[8,4,128]{2,1,0:T(4,128)(2,1)S(1)}, bf16[8,4,128,256]{3,2,1,0:T(8,128)(2,1)}, /*index=5*/s32[]{:T(128)}, s32[]{:T(128)}, s32[]{:T(128)}) while((s32[]{:T(128)}, f32[4,128,256]{2,1,0:T(8,128)S(1)}, s32[]{:T(128)}, bf16[8,4,128]{2,1,0:T(4,128)(2,1)S(1)}, ...), condition=%wide.region_4.5_spmd, body=%wide.region_3.4_spmd.sunk | while | flops 393733 | bytes 1315975 | solution.py:28
  314.1 1.1 convert_add_fusion.2
  315.2 1.1 convert_add_fusion.2
  316.4 1.1 convert_add_fusion.2
  317.5 1.1 convert_add_fusion.2
  321.2 7.4 %fusion.3 = f32[16,4,256,64]{2,3,1,0:T(8,128)} fusion(f32[16,4,128,256]{3,2,1,0:T(8,128)} %get-tuple-element.86, f32[16,4,128]{2,1,0:T(4,128)S(1)} %get-tuple-element.90, f32[4,128,256]{2,1,0:T(8,128)S(1)} %get-tuple-element.89, bf16[16,64,4,128]{3,0,1,2:T(8,128)(2,1)} %get-tuple-element.162), kind=kOutput, calls=%fused_computation.18 | convolution fusion | flops 274726912 | bytes 14188544 | tf_op jit(solution)/shard_map/nihd,nhde->nihe/dot_general | solution.py:88
  328.6 6.9 %multiply_reduce_fusion = (f32[16,64,4]{1,2,0:T(4,128)S(1)}, f32[16,64,4,256]{3,1,2,0:T(8,128)}) fusion(f32[16,4,256,64]{2,3,1,0:T(8,128)} %fusion.3, bf16[16,64,4,256]{3,2,1,0:T(4,128)(2,1)} %copy-done.1, bf16[16,64,4,128]{3,0,1,2:T(8,128)(2,1)} %get-tuple-element.160, pred[64,64]{1,0:T(8,128)(4,1)S(1)} %iota_compare_fusion.1, ...), kind=kOutput, calls=%fused_computation.26 | convolution fusion | flops 204992512 | bytes 12603392 | tf_op jit(solution)/shard_map/nhij,njhe->nihe/dot_general | solution.py:86
  335.5 2.6 multiply_convert_fusion
  338.1 1.8 copy.46
  339.9 1.8 copy.57
  341.7 1.2 gather_fusion.1
  342.9 1.3 reshape.217
  344.3 3.2 multiply_reduce_fusion.1
  (136 shorter events, 23.6 us)
Async XLA Ops:
  8.0 246.8 %copy-start = (f32[256,2]{0,1:T(2,128)S(1)}, f32[256,2]{0,1:T(2,128)}, u32[]{:S(2)}) copy-start(f32[256,2]{0,1:T(2,128)} %param.25) | copy-start | bytes 6148
  8.0 145.0 %all-gather.6.cloned.1.call-start = ((), (), s32[]{:S(2)}) async-start(), calls=%async_computation.3 | async-start | bytes 10485760 | tf_op jit(solution)/shard_map/all_gather | solution.py:129
  12.9 24.7 %copy-start.2 = (bf16[256,4096]{1,0:T(8,128)(2,1)S(1)}, bf16[256,4096]{1,0:T(8,128)(2,1)}, u32[]{:S(2)}) copy-start(bf16[256,4096]{1,0:T(8,128)(2,1)} %param.22) | copy-start | bytes 6291460
  12.9 24.7 %copy-start.5 = (f32[4096]{0:T(1024)S(1)}, f32[4096]{0:T(1024)}, u32[]{:S(2)}) copy-start(f32[4096]{0:T(1024)} %param.23) | copy-start | bytes 49156
  93.4 155.4 %reduce-scatter.2.cloned.1.call-start = ((), (), s32[]{:S(2)}) async-start(), calls=%async_computation.4 | async-start | bytes 10485760 | tf_op jit(solution)/shard_map/reduce_scatter | solution.py:138
  101.6 13.4 %copy-start.1 = (bf16[16,64,4,256]{3,2,1,0:T(4,128)(2,1)}, bf16[16,64,4,256]{3,2,1,0:T(4,128)(2,1)S(1)}, u32[]{:S(2)}) copy-start(bf16[16,64,4,256]{3,2,1,0:T(4,128)(2,1)S(1)} %reshape.181) | copy-start | bytes 6291460
  107.8 2.2 copy-start.3
  107.8 2.9 copy-start.4
  177.2 136.8 %all-gather.8.cloned.1.call-start = ((), (), s32[]{:S(2)}) async-start(), calls=%async_computation.5 | async-start | bytes 2359296 | tf_op jit(solution)/shard_map/all_gather | solution.py:14
  248.8 92.9 %all-to-all-start.1 = ((bf16[1,8,32,4096]{3,2,0,1:T(8,128)(2,1)}), bf16[1,8,32,4096]{3,2,0,1:T(8,128)(2,1)S(1)}, u32[]{:S(2)}, u32[]{:S(2)}) async-start(bf16[1,8,32,4096]{3,2,0,1:T(8,128)(2,1)} %bitcast.91), calls=%async_computation.2 | async-start | bytes 4194304 | tf_op jit(solution)/shard_map/all_to_all | solution.py:146
  328.6 6.9 %copy-start.7 = (f32[256]{0:T(256)S(1)}, f32[256]{0:T(256)}, u32[]{:S(2)}) copy-start(f32[256]{0:T(256)} %param.21) | copy-start | bytes 3076
  344.3 3.4 copy-start.6
Sparse Core Ops, SparseCore 0:
  93.5 59.4 all-gather.5
  177.3 71.4 reduce-scatter.1
Sparse Core Ops, SparseCore 1:
  212.8 55.7 all-gather.7
where the time goes:
time: 358 us; the launch traced here: 356 us
  blocking collectives  111 us (31%)
  waiting for transfers between devices  69.4 us (19%)
  other arithmetic  61.8 us (17%)
  local copies, waits for them, and re-layouts  48.5 us (14%)
  matrix products  42.9 us (12%)
  between operations  15.8 us (4%)
  starting transfers between devices  6.13 us (2%)
    all_gather x1, blocking collectives, entering(): lax.all_gather(a.astype(kind), axis)  58.9 us
    all_to_all x1, blocking collectives, routed_experts(): lax.all_to_all(outgoing, 'ep', split_axis=1, concat_axis=1, tiled=True)  51.7 us
    reduce_scatter x1, waiting for transfers between devices, routed_experts(): lax.psum_scatter(jnp.einsum('pskf,fd->pskd', hidden, down_local, preferre...  35.9 us
    all_gather x1, waiting for transfers between devices, routed_experts(): lax.all_gather(lax.all_to_all(outgoing, 'ep', split_axis=1, concat_axis=1...  33.5 us
    scatter x1, local copies, waits for them, and re-layouts, routed_experts(): table = jnp.full((tp_count, experts * capacity), ep_rows, jnp.int32).at[s...  24.7 us
    add x16, other arithmetic, advance(): carry_state * block_decay[..., None] + block_update  20.1 us
    dot_general x1, matrix products, routed_experts(): jnp.einsum('pskf,fd->pskd', hidden, down_local, preferred_element_type=jn...  16 us
    dynamic_update_slice x32, other arithmetic, token_mixer(): lax.scan(advance, start_carry, (update, step_decay))  13.8 us
  transfers between devices with their start and end apart: 4, of which 2 were waited for; matrix products, arithmetic and copies ran while one was open for 25% of the time, Pallas kernels for 0%

commit v1 on v0

v1 whole, which is shorter than its diff:
```python
import functools

import jax
import jax.numpy as jnp
from jax import lax
from jax.experimental import pallas as pl
from jax.experimental.pallas import tpu as pltpu
from jax.sharding import PartitionSpec as P

DK = 128
DV = 256
BLK = 64
CHUNK = 256
GROUPS = 4


def row_norm(values, gain):
    return values * lax.rsqrt(jnp.mean(values * values, axis=-1, keepdims=True) + 1e-06) * gain


def log_rate_of(logit):
    return (jnp.minimum(logit, 0.0) - jnp.log1p(jnp.exp(-jnp.abs(logit)))) * (1.0 / 16.0)


def ordered_sum(mask, values):
    return jnp.dot(
        mask.astype(jnp.float32),
        values,
        precision=lax.Precision.HIGHEST,
        preferred_element_type=jnp.float32,
    )


def summary_kernel(heads, key_ref, value_ref, logit_ref, state_ref, decay_ref, total):
    step = pl.program_id(0)
    rows = key_ref.shape[0]

    @pl.when(step == 0)
    def _():
        state_ref[...] = jnp.zeros_like(state_ref)
        total[...] = jnp.zeros_like(total)

    rate = log_rate_of(logit_ref[...])
    row = lax.broadcasted_iota(jnp.int32, (rows, rows), 0)
    col = lax.broadcasted_iota(jnp.int32, (rows, rows), 1)
    after = ordered_sum(col > row, rate)
    ending = after[0:1] + rate[0:1]
    key_to_end = (key_ref[...].astype(jnp.float32) * jnp.exp(after)).astype(jnp.bfloat16)
    fall = jnp.exp(ending)
    for head in range(heads):
        keys = slice(head * DK, (head + 1) * DK)
        update = lax.dot_general(
            value_ref[:, head * DV : (head + 1) * DV],
            key_to_end[:, keys],
            (((0,), (0,)), ((), ())),
            preferred_element_type=jnp.float32,
        )
        state_ref[head] = state_ref[head] * fall[:, keys] + update
    total[...] += ending
    decay_ref[...] = jnp.exp(total[...])


def mixer_kernel(
    heads, query_ref, key_ref, value_ref, logit_ref, start_ref, gain_ref, out_ref, state
):
    @pl.when(pl.program_id(0) == 0)
    def _():
        state[...] = start_ref[...]

    rows = key_ref.shape[0]
    rate = log_rate_of(logit_ref[...])
    row = lax.broadcasted_iota(jnp.int32, (rows, rows), 0)
    col = lax.broadcasted_iota(jnp.int32, (rows, rows), 1)
    cumulative = ordered_sum((col <= row) & (col // BLK == row // BLK), rate)
    query_decay = (query_ref[...].astype(jnp.float32) * jnp.exp(cumulative)).astype(jnp.bfloat16)
    keys_wide = key_ref[...].astype(jnp.float32)
    key_decay = (keys_wide * jnp.exp(-cumulative)).astype(jnp.bfloat16)
    causal = lax.broadcasted_iota(jnp.int32, (BLK, BLK), 1) <= lax.broadcasted_iota(
        jnp.int32, (BLK, BLK), 0
    )
    gain = gain_ref[...]
    for block in range(rows // BLK):
        here = slice(block * BLK, (block + 1) * BLK)
        part = cumulative[here]
        ending = part[BLK - 1 : BLK]
        key_to_end = (keys_wide[here] * jnp.exp(ending - part)).astype(jnp.bfloat16)
        fall = jnp.exp(ending)
        for head in range(heads):
            keys = slice(head * DK, (head + 1) * DK)
            values = value_ref[here, head * DV : (head + 1) * DV]
            scores = lax.dot_general(
                query_decay[here, keys],
                key_decay[here, keys],
                (((1,), (1,)), ((), ())),
                preferred_element_type=jnp.float32,
            )
            weights = jnp.where(causal, scores, 0.0).astype(jnp.bfloat16)
            inside = jnp.dot(weights, values, preferred_element_type=jnp.float32)
            before = state[head]
            carried = lax.dot_general(
                query_decay[here, keys],
                before.astype(jnp.bfloat16),
                (((1,), (1,)), ((), ())),
                preferred_element_type=jnp.float32,
            )
            update = lax.dot_general(
                values,
                key_to_end[:, keys],
                (((0,), (0,)), ((), ())),
                preferred_element_type=jnp.float32,
            )
            state[head] = before * fall[:, keys] + update
            out_ref[here, head * DV : (head + 1) * DV] = row_norm(inside + carried, gain).astype(
                out_ref.dtype
            )


def entering(decay, state):
    ep_count = lax.axis_size("ep")
    place = lax.axis_index("ep")

    def from_earlier(value, distance):
        pairs = [(i, i + distance) for i in range(ep_count - distance)]
        return lax.ppermute(value, "ep", pairs)

    def moved(pair, distance):
        fall, held = pair
        fall = from_earlier(fall.astype(jnp.bfloat16), distance).astype(jnp.float32)
        held = from_earlier(held.astype(jnp.bfloat16), distance).astype(jnp.float32)
        return (jnp.where(place >= distance, fall, 1.0), held)

    def join(earlier, later):
        return (earlier[0] * later[0], earlier[1] * later[0][:, None, :] + later[1])

    own = (decay, state)
    window = moved(own, 1)
    distance = 2
    while distance < ep_count:
        window = join(moved(join(window, own), distance), window)
        distance *= 2
    return window[1]


def token_mixer(queries, key_vectors, value_vectors, decay_logit, head_gain):
    positions = queries.shape[0]
    heads = queries.shape[1] // DK
    chunk = CHUNK if positions % CHUNK == 0 else BLK
    steps = positions // chunk

    def rows_of(width):
        return pl.BlockSpec((chunk, width), lambda n: (n, 0))

    def whole(shape):
        return pl.BlockSpec(shape, lambda n: (0,) * len(shape))

    key_width, value_width = heads * DK, heads * DV
    order = pltpu.CompilerParams(dimension_semantics=("arbitrary",))
    state, decay = pl.pallas_call(
        functools.partial(summary_kernel, heads),
        grid=(steps,),
        in_specs=[rows_of(key_width), rows_of(value_width), rows_of(key_width)],
        out_specs=[whole((heads, DV, DK)), whole((1, key_width))],
        out_shape=[
            jax.ShapeDtypeStruct((heads, DV, DK), jnp.float32),
            jax.ShapeDtypeStruct((1, key_width), jnp.float32),
        ],
        scratch_shapes=[pltpu.VMEM((1, key_width), jnp.float32)],
        compiler_params=order,
        cost_estimate=pl.CostEstimate(
            flops=4000000000, bytes_accessed=positions * heads * 1280, transcendentals=2000000
        ),
        name="summary",
    )(key_vectors, value_vectors, decay_logit)
    start = entering(decay.reshape(heads, DK), state)
    return pl.pallas_call(
        functools.partial(mixer_kernel, heads),
        grid=(steps,),
        in_specs=[
            rows_of(key_width),
            rows_of(key_width),
            rows_of(value_width),
            rows_of(key_width),
            whole((heads, DV, DK)),
            whole((1, DV)),
        ],
        out_specs=rows_of(value_width),
        out_shape=jax.ShapeDtypeStruct((positions, value_width), jnp.bfloat16),
        scratch_shapes=[pltpu.VMEM((heads, DV, DK), jnp.float32)],
        compiler_params=order,
        cost_estimate=pl.CostEstimate(
            flops=16000000000, bytes_accessed=positions * heads * 2048, transcendentals=4000000
        ),
        name="mixer",
    )(queries, key_vectors, value_vectors, decay_logit, start, head_gain.reshape(1, DV))


def routed_pairs(
    routed_rows, pre_gain, expert_pick, route_weight, gate_weight, up_weight, down_weight, post_gain
):
    tp_count = lax.axis_size("tp")
    ep_count = lax.axis_size("ep")
    part_index = lax.axis_index("tp")
    place = lax.axis_index("ep")
    ep_rows, width = routed_rows.shape
    part_rows = ep_rows // tp_count
    top_count = expert_pick.shape[1]
    members = ep_count // GROUPS
    room = 2 * top_count * part_rows // ep_count
    along = [[m + g * members for g in range(GROUPS)] for m in range(members)]
    plane_size = members * tp_count
    planes = [[g * plane_size + i for i in range(plane_size)] for g in range(GROUPS)]
    my_group = place // members

    own_rows = lax.dynamic_slice_in_dim(routed_rows, part_index * part_rows, part_rows, 0)
    normed = row_norm(own_rows.astype(jnp.float32), pre_gain).astype(jnp.bfloat16)
    seen = lax.all_gather(normed, "ep", axis_index_groups=along)

    notes = jnp.concatenate([expert_pick.astype(jnp.float32).T, route_weight.T], axis=0)
    notes = lax.all_gather(notes, "ep").reshape(
        GROUPS, members, 2 * top_count, tp_count, part_rows
    )
    notes = notes.transpose(1, 3, 0, 2, 4)
    picks, shares = notes[..., :top_count, :], notes[..., top_count:, :]
    group_of = jnp.floor(picks[..., 0, :] / members).astype(jnp.int32)

    def slots_of(mine):
        order = jnp.cumsum(mine.astype(jnp.int32), axis=-1) - 1
        slot = jnp.arange(room, dtype=jnp.int32)[:, None]
        return mine[..., None, :] & (order[..., None, :] == slot)

    table = slots_of(group_of == my_group)
    share = jnp.sum(jnp.where(picks == place.astype(jnp.float32), shares, 0.0), axis=-2)
    slot_share = jnp.sum(jnp.where(table, share[..., None, :], 0.0), axis=-1).reshape(-1, 1)

    own_table = lax.dynamic_index_in_dim(
        lax.dynamic_index_in_dim(table, place % members, 0, False), part_index, 0, False
    )
    chosen = jnp.einsum(
        "gsr,grd->gsd",
        own_table.astype(jnp.bfloat16),
        seen,
        preferred_element_type=jnp.float32,
    ).astype(jnp.bfloat16)
    arrived = lax.all_gather(
        chosen.reshape(GROUPS * room, width),
        ("ep", "tp"),
        axis_index_groups=planes,
        tiled=True,
    )
    gate_act = jnp.dot(arrived, gate_weight[0], preferred_element_type=jnp.float32)
    up_act = jnp.dot(arrived, up_weight[0], preferred_element_type=jnp.float32)
    hidden = (jax.nn.silu(gate_act) * up_act).astype(jnp.bfloat16)
    product = jnp.dot(hidden, down_weight[0], preferred_element_type=jnp.float32)
    summed = lax.psum_scatter(
        (product * slot_share).astype(jnp.bfloat16),
        ("ep", "tp"),
        scatter_dimension=0,
        axis_index_groups=planes,
        tiled=True,
    )
    returned = lax.all_to_all(
        summed.reshape(GROUPS, room, width),
        "ep",
        split_axis=0,
        concat_axis=0,
        axis_index_groups=along,
        tiled=True,
    )
    own_picks = lax.dynamic_slice_in_dim(expert_pick, part_index * part_rows, part_rows, 0)
    own_group = own_picks[:, 0] // members
    places = slots_of(own_group[None, :] == jnp.arange(GROUPS, dtype=jnp.int32)[:, None])
    combined = jnp.einsum(
        "gsr,gsd->rd", places.astype(jnp.bfloat16), returned, preferred_element_type=jnp.float32
    )
    return row_norm(combined, post_gain).astype(jnp.bfloat16)


def routed_any(
    routed_rows, pre_gain, expert_pick, route_weight, gate_weight, up_weight, down_weight, post_gain
):
    tp_count = lax.axis_size("tp")
    ep_count = lax.axis_size("ep")
    part_index = lax.axis_index("tp")
    ep_rows, model_width = routed_rows.shape
    part_rows = ep_rows // tp_count
    top_count = expert_pick.shape[1]
    experts = ep_count * gate_weight.shape[0]
    capacity = 2 * top_count * part_rows // experts
    normed = row_norm(routed_rows.astype(jnp.float32), pre_gain).astype(jnp.bfloat16)
    padded = jnp.concatenate([normed, jnp.zeros((1, model_width), jnp.bfloat16)], axis=0)
    picks = expert_pick.reshape(tp_count, part_rows * top_count)
    matches = (picks[:, :, None] == jnp.arange(experts, dtype=jnp.int32)[None, None, :]).astype(
        jnp.int32
    )
    slots = jnp.sum((jnp.cumsum(matches, axis=1) - 1) * matches, axis=2)
    targets = picks * capacity + slots
    sources = (
        jnp.arange(part_rows * top_count, dtype=jnp.int32)[None, :] // top_count
        + part_rows * jnp.arange(tp_count, dtype=jnp.int32)[:, None]
    )
    slice_offset_index = jnp.broadcast_to(
        jnp.arange(tp_count, dtype=jnp.int32)[:, None], targets.shape
    )
    table = (
        jnp.full((tp_count, experts * capacity), ep_rows, jnp.int32)
        .at[slice_offset_index, targets]
        .set(sources)
    )
    gate_local = gate_weight[0]
    up_local = up_weight[0]
    down_local = down_weight[0]
    own_table = lax.dynamic_slice_in_dim(table, part_index, 1, 0)
    outgoing = padded[own_table].reshape(1, ep_count, capacity, model_width)
    arrived = lax.all_gather(
        lax.all_to_all(outgoing, "ep", split_axis=1, concat_axis=1, tiled=True),
        "tp",
        axis=0,
        tiled=True,
    )
    gate_act = jnp.einsum("pskd,df->pskf", arrived, gate_local, preferred_element_type=jnp.float32)
    up_act = jnp.einsum("pskd,df->pskf", arrived, up_local, preferred_element_type=jnp.float32)
    hidden = (jax.nn.silu(gate_act) * up_act).astype(jnp.bfloat16)
    summed = lax.psum_scatter(
        jnp.einsum("pskf,fd->pskd", hidden, down_local, preferred_element_type=jnp.float32).astype(
            jnp.bfloat16
        ),
        "tp",
        scatter_dimension=0,
        tiled=True,
    )
    returned = lax.all_to_all(summed, "ep", split_axis=1, concat_axis=1, tiled=True)
    flattened = returned.reshape(experts * capacity, model_width)
    my_slots = lax.dynamic_slice_in_dim(targets, part_index, 1, 0).reshape(part_rows, top_count)
    my_weight = lax.dynamic_slice_in_dim(route_weight, part_index * part_rows, part_rows, 0)
    combined = jnp.sum(flattened[my_slots].astype(jnp.float32) * my_weight[:, :, None], axis=1)
    return row_norm(combined, post_gain).astype(jnp.bfloat16)


def routed_experts(
    routed_rows, pre_gain, expert_pick, route_weight, gate_weight, up_weight, down_weight, post_gain
):
    whole_groups = lax.axis_size("ep") == GROUPS * expert_pick.shape[1]
    form = routed_pairs if whole_groups and gate_weight.shape[0] == 1 else routed_any
    return form(
        routed_rows,
        pre_gain,
        expert_pick,
        route_weight,
        gate_weight,
        up_weight,
        down_weight,
        post_gain,
    )


def on_device(
    queries,
    key_vectors,
    value_vectors,
    decay_logit,
    head_gain,
    routed_rows,
    pre_gain,
    expert_pick,
    route_weight,
    gate_weight,
    up_weight,
    down_weight,
    post_gain,
):
    mixed_heads = token_mixer(queries, key_vectors, value_vectors, decay_logit, head_gain)
    routed_out = routed_experts(
        routed_rows,
        pre_gain,
        expert_pick,
        route_weight,
        gate_weight,
        up_weight,
        down_weight,
        post_gain,
    )
    return (mixed_heads, routed_out)


def solution(mesh):
    placed = (
        P("ep", "tp"),
        P("ep", "tp"),
        P("ep", "tp"),
        P("ep", "tp"),
        P(),
        P("ep", None),
        P(),
        P("ep", None),
        P("ep", None),
        P("ep", None, "tp"),
        P("ep", None, "tp"),
        P("ep", "tp", None),
        P(),
    )
    return jax.shard_map(
        on_device,
        mesh=mesh,
        in_specs=placed,
        out_specs=(P("ep", "tp"), P(("ep", "tp"), None)),
        check_vma=False,
    )
```

time: 358 us -> 250 us (0.70)
  blocking collectives: 111 us -> 29 us
  waiting for transfers between devices: 69.4 us -> 124 us
  local copies, waits for them, and re-layouts: 48.5 us -> 0.31 us
  other arithmetic: 61.8 us -> 13.9 us
  Pallas kernels: 0 us -> 22.9 us
  matrix products: 42.9 us -> 27.5 us
  starting transfers between devices: 6.13 us -> 14.4 us
    all_to_all x1 -> x0, blocking collectives: 51.7 us -> none  [routed_experts(): lax.all_to_all(outgoing, 'ep', split_axis=1, concat_axis=1, tiled=True)]
    all_gather x2, waiting for transfers between devices: 33.5 us -> 67.2 us  [the longest x1 54.8 us: routed_pairs(): lax.all_gather(chosen.reshape(GROUPS * room, width), ('ep', 'tp'), axis_i...]
    all_gather x1, blocking collectives: 58.9 us -> 29 us  [routed_pairs(): lax.all_gather(notes, 'ep')]
    add x24 -> x1, other arithmetic: 26.8 us -> 0.92 us  [join(): return (earlier[0] * later[0], earlier[1] * later[0][:, None, :] + later[1])]
    scatter x1 -> x0, local copies, waits for them, and re-layouts: 24.7 us -> none  [routed_experts(): table = jnp.full((tp_count, experts * capacity), ep_rows, jnp.int32).at[s...]
    pallas_call x0 -> x2, Pallas kernels: none -> 22.9 us  [the longest x1 15.9 us: token_mixer(): pl.pallas_call(functools.partial(mixer_kernel, heads), grid=(steps,), in_...]
    dot_general x5 -> x4, matrix products: 42.9 us -> 27.5 us  [the longest x1 15.9 us: routed_pairs(): jnp.dot(hidden, down_weight[0], preferred_element_type=jnp.float32)]
    ppermute x0 -> x5, waiting for transfers between devices: none -> 15 us  [from_earlier(): return lax.ppermute(value, 'ep', pairs)]
  transfers between devices with their start and end apart: 4 -> 9, of which waited for: 2 -> 6; matrix products, arithmetic and copies ran while one was open for 25% -> 4% of each run, Pallas kernels for 0% -> 9%
where the time goes in v1:
time: 250 us; the launch traced here: 246 us
  waiting for transfers between devices  124 us (50%)
  blocking collectives  29 us (12%)
  matrix products  27.5 us (11%)
  Pallas kernels  22.9 us (9%)
  starting transfers between devices  14.4 us (6%)
  other arithmetic  13.9 us (6%)
  between operations  13.9 us (6%)
    all_gather x1, waiting for transfers between devices, routed_pairs(): lax.all_gather(chosen.reshape(GROUPS * room, width), ('ep', 'tp'), axis_i...  54.8 us
    reduce_scatter x1, waiting for transfers between devices, routed_pairs(): lax.psum_scatter((product * slot_share).astype(jnp.bfloat16), ('ep', 'tp'...  35.3 us
    all_gather x1, blocking collectives, routed_pairs(): lax.all_gather(notes, 'ep')  29 us
    dot_general x1, matrix products, routed_pairs(): jnp.dot(hidden, down_weight[0], preferred_element_type=jnp.float32)  15.9 us
    pallas_call x1, Pallas kernels, token_mixer(): pl.pallas_call(functools.partial(mixer_kernel, heads), grid=(steps,), in_...  15.9 us
    ppermute x5, waiting for transfers between devices, from_earlier(): return lax.ppermute(value, 'ep', pairs)  15 us
    all_gather x1, waiting for transfers between devices, routed_pairs(): seen = lax.all_gather(normed, 'ep', axis_index_groups=along)  12.4 us
    ppermute x5, starting transfers between devices, from_earlier(): return lax.ppermute(value, 'ep', pairs)  9.15 us
  transfers between devices with their start and end apart: 9, of which 6 were waited for; matrix products, arithmetic and copies ran while one was open for 4% of the time, Pallas kernels for 9%

profile of v1, /device:TPU:24, one launch (start us, length us, event | category | flops | bytes accessed | tf_op | source)
XLA Modules:
  0.0 245.8 jit_solution(584429076563067887)
XLA Ops:
  7.2 0.0 all-gather.8.cloned.1.call-start
  7.2 1.2 fusion.9
  8.5 2.0 fusion.11
  10.5 0.0 all-gather.8.cloned.1.call-update
  10.6 0.0 all-gather.6.cloned.1.call-start
  10.6 0.7 convert_bitcast_fusion
  11.3 0.7 maximum_bitcast_fusion
  12.0 29.0 %all-gather.2 = f32[8,4,256]{2,1,0:T(4,128)S(1)} all-gather(f32[1,4,256]{2,1,0:T(4,128)S(1)} %maximum_bitcast_fusion), channel_id=2, replica_groups=mesh['ep'=8,'tp'=4] {'ep'}, dimensions={0}, use_global_device_ids=true | all-gather | bytes 36864 | tf_op jit(solution)/shard_map/all_gather | solution.py:219
  41.0 0.1 reshape.116
  41.2 1.9 reduce_window_sum.26
  43.1 0.1 fusion.15
  43.2 12.4 %all-gather.8.cloned.1.call-done = bf16[256,4096]{1,0:T(8,128)(2,1)} async-done(((bf16[64,4096]{1,0:T(8,128)(2,1)}), bf16[256,4096]{1,0:T(8,128)(2,1)}) %all-gather.8.cloned.1.call-update) | async-done | bytes 2097168 | tf_op jit(solution)/shard_map/all_gather | solution.py:216
  55.6 3.0 %convolution_convert_fusion = bf16[4,32,4096]{2,1,0:T(8,128)(2,1)} fusion(bf16[4,64,4096]{2,1,0:T(8,128)(2,1)} %bitcast.47, pred[2,4,4,32,64]{4,3,2,1,0:T(32,128)(4,1)S(1)} %fusion.15, s32[]{:T(128)S(6)} %select_n.67, s32[]{:T(128)S(6)} %select_n.69), kind=kOutput, calls=%fused_computation.1 | convolution fusion | flops 67633152 | bytes 3162120 | tf_op jit(solution)/shard_map/gsr,grd->gsd/dot_general | solution.py:238
  58.6 0.0 all-gather.6.cloned.1.call-update
  58.6 0.0 reduce-scatter.2.cloned.1.call-start
  58.7 0.2 select_reduce_fusion
  58.9 0.1 mul.115
  59.0 54.8 %all-gather.6.cloned.1.call-done = bf16[1024,4096]{1,0:T(8,128)(2,1)} async-done(((bf16[128,4096]{1,0:T(8,128)(2,1)}), bf16[1024,4096]{1,0:T(8,128)(2,1)}) %all-gather.6.cloned.1.call-update) | async-done | bytes 8388624 | tf_op jit(solution)/shard_map/all_gather | solution.py:244
  113.8 8.1 %fusion.3 = f32[1024,512]{1,0:T(8,128)S(1)} fusion(bf16[1024,4096]{1,0:T(8,128)(2,1)} %all-gather.6.cloned.1.call-done, bf16[1,4096,512]{2,1,0:T(8,128)(2,1)} %param.22), kind=kOutput, calls=%fused_computation.6 | convolution fusion | flops 4294967296 | bytes 14680064 | tf_op jit(solution)/shard_map/dot_general | solution.py:250
  121.9 15.9 %multiply_convert_fusion = bf16[1024,4096]{1,0:T(8,128)(2,1)} fusion(f32[1024]{0:T(1024)S(1)} %mul.115, bf16[1,512,4096]{2,1,0:T(8,128)(2,1)} %param.24, f32[1024,512]{1,0:T(8,128)S(1)} %fusion.3, bf16[1024,4096]{1,0:T(8,128)(2,1)} %all-gather.6.cloned.1.call-done, bf16[1,4096,512]{2,1,0:T(8,128)(2,1)} %param.23), kind=kOutput, calls=%fused_computation | convolution fusion | flops 8601468928 | bytes 27267072 | tf_op jit(solution)/shard_map/dot_general | solution.py:253
  137.9 0.0 reduce-scatter.2.cloned.1.call-update
  137.9 0.0 copy-start.1
  137.9 7.0 %summary.1 = (f32[4,256,128]{2,1,0:T(8,128)}, f32[1,512]{1,0:T(1,128)}) custom-call(bf16[1024,512]{1,0:T(8,128)(2,1)} %key_ref.3, bf16[1024,1024]{1,0:T(8,128)(2,1)} %value_ref.3, f32[1024,512]{1,0:T(8,128)} %logit_ref.3), custom_call_target="tpu_custom_call" | custom-call | flops 4000000000 | bytes 5242880 | tf_op jit(solution)/shard_map/summary/pallas_call | solution.py:158
  144.9 0.7 convert_element_type.74
  145.6 3.4 %collective-permute-start.2 = (bf16[4,128]{1,0:T(4,128)(2,1)S(1)}, bf16[4,128]{1,0:T(4,128)(2,1)S(1)}, u32[]{:S(2)}, u32[]{:S(2)}) collective-permute-start(bf16[4,128]{1,0:T(4,128)(2,1)S(1)} %convert_element_type.74), channel_id=1, source_target_pairs={{0,4},{4,8},{8,12},{12,16},{16,20},{20,24},{24,28},{1,5},{5,9},{9,... | collective-permute-start | bytes 3080 | tf_op jit(solution)/shard_map/ppermute | solution.py:124
  149.0 1.1 convert_element_type.70
  150.1 1.9 collective-permute-start
  152.0 0.0 copy-done.1
  152.0 0.1 constant_dynamic-slice_fusion
  152.1 0.0 collective-permute-done.2
  152.1 0.7 multiply_convert_fusion.3
  152.8 1.3 collective-permute-start.4
  154.1 7.0 %collective-permute-done = bf16[4,256,128]{2,1,0:T(8,128)(2,1)S(1)} collective-permute-done((bf16[4,256,128]{2,1,0:T(8,128)(2,1)S(1)}, bf16[4,256,128]{2,1,0:T(8,128)(2,1)S(1)}, u32[]{:S(2)}, u32[]{:S(2)}) %collective-permute-start) | collective-permute-done | bytes 262176 | tf_op jit(solution)/shard_map/ppermute | solution.py:124
  161.2 1.1 fusion.14
  162.3 1.3 collective-permute-start.1
  163.6 0.0 collective-permute-done.4
  163.6 7.9 %collective-permute-done.1 = bf16[4,256,128]{2,1,0:T(8,128)(2,1)S(1)} collective-permute-done((bf16[4,256,128]{2,1,0:T(8,128)(2,1)S(1)}, bf16[4,256,128]{2,1,0:T(8,128)(2,1)S(1)}, u32[]{:S(2)}, u32[]{:S(2)}) %collective-permute-start.1) | collective-permute-done | bytes 262176 | tf_op jit(solution)/shard_map/ppermute | solution.py:124
  171.5 1.2 add_convert_fusion
  172.7 1.3 collective-permute-start.3
  174.0 0.2 reduce_window_sum.24
  174.3 35.3 %reduce-scatter.2.cloned.1.call-done = bf16[128,4096]{1,0:T(8,128)(2,1)} async-done(((bf16[1024,4096]{1,0:T(8,128)(2,1)}), bf16[128,4096]{1,0:T(8,128)(2,1)}) %reduce-scatter.2.cloned.1.call-update) | async-done | bytes 1048592 | tf_op jit(solution)/shard_map/reduce_scatter | solution.py:254
  209.5 5.1 %all-to-all-start = ((bf16[4,32,4096]{2,1,0:T(8,128)(2,1)}), bf16[4,32,4096]{2,1,0:T(8,128)(2,1)S(1)}, u32[]{:S(2)}, u32[]{:S(2)}) async-start(bf16[4,32,4096]{2,1,0:T(8,128)(2,1)} %bitcast.48), calls=%async_computation.1 | async-start | bytes 2097152 | tf_op jit(solution)/shard_map/all_to_all | solution.py:261
  214.6 0.0 collective-permute-done.3
  214.6 0.9 multiply_add_fusion.start_ref
  215.5 15.9 %mixer.1 = bf16[1024,1024]{1,0:T(8,128)(2,1)} custom-call(bf16[1024,512]{1,0:T(8,128)(2,1)} %query_ref.1, bf16[1024,512]{1,0:T(8,128)(2,1)} %key_ref.3, bf16[1024,1024]{1,0:T(8,128)(2,1)} %value_ref.3, f32[1024,512]{1,0:T(8,128)} %logit_ref.3, f32[4,256,128]{2,1,0:T(8,128)} %multiply_add_fusion.start_ref, f32[1,256]{1,0:T(1,128)} %bitcast.56), custom_call_target="tpu_custom_call" | custom-call | flops 16000000000 | bytes 8388608 | tf_op jit(solution)/shard_map/mixer/pallas_call | solution.py:175
  231.5 6.3 %all-to-all-done = bf16[4,32,4096]{2,1,0:T(8,128)(2,1)S(1)} async-done(((bf16[4,32,4096]{2,1,0:T(8,128)(2,1)}), bf16[4,32,4096]{2,1,0:T(8,128)(2,1)S(1)}, u32[]{:S(2)}, u32[]{:S(2)}) %all-to-all-start) | async-done | bytes 1048608 | tf_op jit(solution)/shard_map/all_to_all | solution.py:261
  237.8 0.5 multiply_reduce_fusion
  238.3 1.0 multiply_convert_fusion.2
  (12 shorter events, 0.1 us)
Async XLA Ops:
  7.2 48.4 %all-gather.8.cloned.1.call-start = ((), (), s32[]{:S(2)}) async-start(), calls=%async_computation.4 | async-start | bytes 2621440 | tf_op jit(solution)/shard_map/all_gather | solution.py:216
  10.6 103.2 %all-gather.6.cloned.1.call-start = ((), (), s32[]{:S(2)}) async-start(), calls=%async_computation.2 | async-start | bytes 9437184 | tf_op jit(solution)/shard_map/all_gather | solution.py:244
  58.6 150.9 %reduce-scatter.2.cloned.1.call-start = ((), (), s32[]{:S(2)}) async-start(), calls=%async_computation.3 | async-start | bytes 9437184 | tf_op jit(solution)/shard_map/reduce_scatter | solution.py:254
  137.9 14.2 %copy-start.1 = (s32[256,2]{0,1:T(2,128)S(1)}, s32[256,2]{0,1:T(2,128)}, u32[]{:S(2)}) copy-start(s32[256,2]{0,1:T(2,128)} %param.20) | copy-start | bytes 6148
  145.6 6.5 %collective-permute-start.2 = (bf16[4,128]{1,0:T(4,128)(2,1)S(1)}, bf16[4,128]{1,0:T(4,128)(2,1)S(1)}, u32[]{:S(2)}, u32[]{:S(2)}) collective-permute-start(bf16[4,128]{1,0:T(4,128)(2,1)S(1)} %convert_element_type.74), channel_id=1, source_target_pairs={{0,4},{4,8},{8,12},{12,16},{16,20},{20,24},{24,28},{1,5},{5,9},{9,... | collective-permute-start | bytes 3080 | tf_op jit(solution)/shard_map/ppermute | solution.py:124
  150.1 11.1 %collective-permute-start = (bf16[4,256,128]{2,1,0:T(8,128)(2,1)S(1)}, bf16[4,256,128]{2,1,0:T(8,128)(2,1)S(1)}, u32[]{:S(2)}, u32[]{:S(2)}) collective-permute-start(bf16[4,256,128]{2,1,0:T(8,128)(2,1)S(1)} %convert_element_type.70), channel_id=1, source_target_pairs={{0,4},{4,8},{8,12},{12,16},{16,20},{20,24},{24,28},{1,5},{5,9},{9,... | collective-permute-start | bytes 786440 | tf_op jit(solution)/shard_map/ppermute | solution.py:124
  152.8 10.8 %collective-permute-start.4 = (bf16[4,128]{1,0:T(4,128)(2,1)S(1)}, bf16[4,128]{1,0:T(4,128)(2,1)S(1)}, u32[]{:S(2)}, u32[]{:S(2)}) collective-permute-start(bf16[4,128]{1,0:T(4,128)(2,1)S(1)} %multiply_convert_fusion.3), channel_id=1, source_target_pairs={{0,8},{4,12},{8,16},{12,20},{16,24},{20,28},{1,9},{5,13},{9,17},{1... | collective-permute-start | bytes 3080 | tf_op jit(solution)/shard_map/ppermute | solution.py:124
  162.3 9.3 %collective-permute-start.1 = (bf16[4,256,128]{2,1,0:T(8,128)(2,1)S(1)}, bf16[4,256,128]{2,1,0:T(8,128)(2,1)S(1)}, u32[]{:S(2)}, u32[]{:S(2)}) collective-permute-start(bf16[4,256,128]{2,1,0:T(8,128)(2,1)S(1)} %fusion.14), channel_id=1, source_target_pairs={{0,8},{4,12},{8,16},{12,20},{16,24},{20,28},{1,9},{5,13},{9,17},{1... | collective-permute-start | bytes 786440 | tf_op jit(solution)/shard_map/ppermute | solution.py:124
  172.7 41.9 %collective-permute-start.3 = (bf16[4,256,128]{2,1,0:T(8,128)(2,1)S(1)}, bf16[4,256,128]{2,1,0:T(8,128)(2,1)S(1)}, u32[]{:S(2)}, u32[]{:S(2)}) collective-permute-start(bf16[4,256,128]{2,1,0:T(8,128)(2,1)S(1)} %add_convert_fusion), channel_id=1, source_target_pairs={{0,16},{4,20},{8,24},{12,28},{1,17},{5,21},{9,25},{13,29},{2,18},{... | collective-permute-start | bytes 786440 | tf_op jit(solution)/shard_map/ppermute | solution.py:124
  209.5 28.3 %all-to-all-start = ((bf16[4,32,4096]{2,1,0:T(8,128)(2,1)}), bf16[4,32,4096]{2,1,0:T(8,128)(2,1)S(1)}, u32[]{:S(2)}, u32[]{:S(2)}) async-start(bf16[4,32,4096]{2,1,0:T(8,128)(2,1)} %bitcast.48), calls=%async_computation.1 | async-start | bytes 2097152 | tf_op jit(solution)/shard_map/all_to_all | solution.py:261
  215.5 22.7 %copy-start = (f32[4096]{0:T(1024)S(1)}, f32[4096]{0:T(1024)}, u32[]{:S(2)}) copy-start(f32[4096]{0:T(1024)} %param.25) | copy-start | bytes 49156
Sparse Core Ops, SparseCore 0:
  10.7 44.8 all-gather.7
  58.7 55.0 all-gather.5
  138.0 71.4 reduce-scatter.1

commit v2 on v1

--- a/solution.py
+++ b/solution.py
@@ -141,52 +141,62 @@
     return window[1]
 
 
-def token_mixer(queries, key_vectors, value_vectors, decay_logit, head_gain):
-    positions = queries.shape[0]
-    heads = queries.shape[1] // DK
+def rows_of(chunk, width):
+    return pl.BlockSpec((chunk, width), lambda n: (n, 0))
+
+
+def whole(shape):
+    return pl.BlockSpec(shape, lambda n: (0,) * len(shape))
+
+
+def sizes_of(keys):
+    positions, key_width = keys.shape
+    heads = key_width // DK
     chunk = CHUNK if positions % CHUNK == 0 else BLK
-    steps = positions // chunk
-
-    def rows_of(width):
-        return pl.BlockSpec((chunk, width), lambda n: (n, 0))
-
-    def whole(shape):
-        return pl.BlockSpec(shape, lambda n: (0,) * len(shape))
-
-    key_width, value_width = heads * DK, heads * DV
-    order = pltpu.CompilerParams(dimension_semantics=("arbitrary",))
+    return positions, heads, chunk, key_width, heads * DV
+
+
+ORDER = pltpu.CompilerParams(dimension_semantics=("arbitrary",))
+
+
+def starting_state(key_vectors, value_vectors, decay_logit):
+    positions, heads, chunk, key_width, value_width = sizes_of(key_vectors)
     state, decay = pl.pallas_call(
         functools.partial(summary_kernel, heads),
-        grid=(steps,),
-        in_specs=[rows_of(key_width), rows_of(value_width), rows_of(key_width)],
+        grid=(positions // chunk,),
+        in_specs=[rows_of(chunk, key_width), rows_of(chunk, value_width), rows_of(chunk, key_width)],
         out_specs=[whole((heads, DV, DK)), whole((1, key_width))],
         out_shape=[
             jax.ShapeDtypeStruct((heads, DV, DK), jnp.float32),
             jax.ShapeDtypeStruct((1, key_width), jnp.float32),
         ],
         scratch_shapes=[pltpu.VMEM((1, key_width), jnp.float32)],
-        compiler_params=order,
+        compiler_params=ORDER,
         cost_estimate=pl.CostEstimate(
             flops=4000000000, bytes_accessed=positions * heads * 1280, transcendentals=2000000
         ),
         name="summary",
     )(key_vectors, value_vectors, decay_logit)
-    start = entering(decay.reshape(heads, DK), state)
+    return entering(decay.reshape(heads, DK), state)
+
+
+def token_mixer(queries, key_vectors, value_vectors, decay_logit, head_gain, start):
+    positions, heads, chunk, key_width, value_width = sizes_of(queries)
     return pl.pallas_call(
         functools.partial(mixer_kernel, heads),
-        grid=(steps,),
+        grid=(positions // chunk,),
         in_specs=[
-            rows_of(key_width),
-            rows_of(key_width),
-            rows_of(value_width),
-            rows_of(key_width),
+            rows_of(chunk, key_width),
+            rows_of(chunk, key_width),
+            rows_of(chunk, value_width),
+            rows_of(chunk, key_width),
             whole((heads, DV, DK)),
             whole((1, DV)),
         ],
-        out_specs=rows_of(value_width),
+        out_specs=rows_of(chunk, value_width),
         out_shape=jax.ShapeDtypeStruct((positions, value_width), jnp.bfloat16),
         scratch_shapes=[pltpu.VMEM((heads, DV, DK), jnp.float32)],
-        compiler_params=order,
+        compiler_params=ORDER,
         cost_estimate=pl.CostEstimate(
             flops=16000000000, bytes_accessed=positions * heads * 2048, transcendentals=4000000
         ),
@@ -195,7 +205,15 @@
 
 
 def routed_pairs(
-    routed_rows, pre_gain, expert_pick, route_weight, gate_weight, up_weight, down_weight, post_gain
+    routed_rows,
+    pre_gain,
+    expert_pick,
+    route_weight,
+    gate_weight,
+    up_weight,
+    down_weight,
+    post_gain,
+    start,
 ):
     tp_count = lax.axis_size("tp")
     ep_count = lax.axis_size("ep")
@@ -213,7 +231,6 @@
 
     own_rows = lax.dynamic_slice_in_dim(routed_rows, part_index * part_rows, part_rows, 0)
     normed = row_norm(own_rows.astype(jnp.float32), pre_gain).astype(jnp.bfloat16)
-    seen = lax.all_gather(normed, "ep", axis_index_groups=along)
 
     notes = jnp.concatenate([expert_pick.astype(jnp.float32).T, route_weight.T], axis=0)
     notes = lax.all_gather(notes, "ep").reshape(
@@ -230,49 +247,64 @@
 
     table = slots_of(group_of == my_group)
     share = jnp.sum(jnp.where(picks == place.astype(jnp.float32), shares, 0.0), axis=-2)
-    slot_share = jnp.sum(jnp.where(table, share[..., None, :], 0.0), axis=-1).reshape(-1, 1)
-
-    own_table = lax.dynamic_index_in_dim(
-        lax.dynamic_index_in_dim(table, place % members, 0, False), part_index, 0, False
-    )
-    chosen = jnp.einsum(
-        "gsr,grd->gsd",
-        own_table.astype(jnp.bfloat16),
-        seen,
-        preferred_element_type=jnp.float32,
-    ).astype(jnp.bfloat16)
-    arrived = lax.all_gather(
-        chosen.reshape(GROUPS * room, width),
-        ("ep", "tp"),
-        axis_index_groups=planes,
-        tiled=True,
-    )
-    gate_act = jnp.dot(arrived, gate_weight[0], preferred_element_type=jnp.float32)
-    up_act = jnp.dot(arrived, up_weight[0], preferred_element_type=jnp.float32)
-    hidden = (jax.nn.silu(gate_act) * up_act).astype(jnp.bfloat16)
-    product = jnp.dot(hidden, down_weight[0], preferred_element_type=jnp.float32)
-    summed = lax.psum_scatter(
-        (product * slot_share).astype(jnp.bfloat16),
-        ("ep", "tp"),
-        scatter_dimension=0,
-        axis_index_groups=planes,
-        tiled=True,
-    )
-    returned = lax.all_to_all(
-        summed.reshape(GROUPS, room, width),
-        "ep",
-        split_axis=0,
-        concat_axis=0,
-        axis_index_groups=along,
-        tiled=True,
-    )
+    slot_share = jnp.sum(jnp.where(table, share[..., None, :], 0.0), axis=-1)
+
     own_picks = lax.dynamic_slice_in_dim(expert_pick, part_index * part_rows, part_rows, 0)
     own_group = own_picks[:, 0] // members
-    places = slots_of(own_group[None, :] == jnp.arange(GROUPS, dtype=jnp.int32)[:, None])
+    places = slots_of(own_group[None, :] == jnp.arange(GROUPS, dtype=jnp.int32)[:, None]).astype(
+        jnp.bfloat16
+    )
+    leaving = jnp.einsum(
+        "gsr,rd->gsd", places, normed, preferred_element_type=jnp.float32
+    ).astype(jnp.bfloat16)
+    chosen = lax.all_to_all(
+        leaving, "ep", split_axis=0, concat_axis=0, axis_index_groups=along, tiled=True
+    )
+    spans = 2 if room % 16 == 0 else 1
+    span = room // spans
+    slot_share = slot_share.reshape(plane_size, GROUPS, spans, span)
+
+    def gathered(turn):
+        return lax.all_gather(
+            chosen[:, turn * span : (turn + 1) * span].reshape(GROUPS * span, width),
+            ("ep", "tp"),
+            axis_index_groups=planes,
+            tiled=True,
+        )
+
+    def experts_on(arrived, turn):
+        gate_act = jnp.dot(arrived, gate_weight[0], preferred_element_type=jnp.float32)
+        up_act = jnp.dot(arrived, up_weight[0], preferred_element_type=jnp.float32)
+        hidden = (jax.nn.silu(gate_act) * up_act).astype(jnp.bfloat16)
+        product = jnp.dot(hidden, down_weight[0], preferred_element_type=jnp.float32)
+        return (product * slot_share[:, :, turn].reshape(-1, 1)).astype(jnp.bfloat16)
+
+    def sent_home(product):
+        summed = lax.psum_scatter(
+            product,
+            ("ep", "tp"),
+            scatter_dimension=0,
+            axis_index_groups=planes,
+            tiled=True,
+        )
+        return lax.all_to_all(
+            summed.reshape(GROUPS, span, width),
+            "ep",
+            split_axis=0,
+            concat_axis=0,
+            axis_index_groups=along,
+            tiled=True,
+        )
+
+    arrivals = [gathered(turn) for turn in range(spans)]
+    arrivals[0], start = lax.optimization_barrier((arrivals[0], start))
+    returned = jnp.concatenate(
+        [sent_home(experts_on(arrived, turn)) for turn, arrived in enumerate(arrivals)], axis=1
+    )
     combined = jnp.einsum(
-        "gsr,gsd->rd", places.astype(jnp.bfloat16), returned, preferred_element_type=jnp.float32
-    )
-    return row_norm(combined, post_gain).astype(jnp.bfloat16)
+        "gsr,gsd->rd", places, returned, preferred_element_type=jnp.float32
+    )
+    return (row_norm(combined, post_gain).astype(jnp.bfloat16), start)
 
 
 def routed_any(
@@ -336,21 +368,12 @@
     return row_norm(combined, post_gain).astype(jnp.bfloat16)
 
 
-def routed_experts(
-    routed_rows, pre_gain, expert_pick, route_weight, gate_weight, up_weight, down_weight, post_gain
-):
+def routed_experts(*operands, start):
+    expert_pick, gate_weight = operands[2], operands[4]
     whole_groups = lax.axis_size("ep") == GROUPS * expert_pick.shape[1]
-    form = routed_pairs if whole_groups and gate_weight.shape[0] == 1 else routed_any
-    return form(
-        routed_rows,
-        pre_gain,
-        expert_pick,
-        route_weight,
-        gate_weight,
-        up_weight,
-        down_weight,
-        post_gain,
-    )
+    if whole_groups and gate_weight.shape[0] == 1:
+        return routed_pairs(*operands, start)
+    return (routed_any(*operands), start)
 
 
 def on_device(
@@ -368,8 +391,8 @@
     down_weight,
     post_gain,
 ):
-    mixed_heads = token_mixer(queries, key_vectors, value_vectors, decay_logit, head_gain)
-    routed_out = routed_experts(
+    start = starting_state(key_vectors, value_vectors, decay_logit)
+    routed_out, start = routed_experts(
         routed_rows,
         pre_gain,
         expert_pick,
@@ -378,6 +401,10 @@
         up_weight,
         down_weight,
         post_gain,
+        start=start,
+    )
+    mixed_heads = token_mixer(
+        queries, key_vectors, value_vectors, decay_logit, head_gain, start
     )
     return (mixed_heads, routed_out)
 

time: 250 us -> 267 us (1.068)
  blocking collectives: 29 us -> 58.2 us
  waiting for transfers between devices: 124 us -> 110 us
  starting transfers between devices: 14.4 us -> 19.7 us
  other arithmetic: 13.9 us -> 10.4 us
    all_gather x2, waiting for transfers between devices: 67.2 us -> 0.01 us  [gathered(): lax.all_gather(chosen[:, turn * span:(turn + 1) * span].reshape(GROUPS *...]
    reduce_scatter x1 -> x2, waiting for transfers between devices: 35.3 us -> 91.8 us  [sent_home(): lax.psum_scatter(product, ('ep', 'tp'), scatter_dimension=0, axis_index_g...]
    all_to_all x0 -> x1, blocking collectives: none -> 28.3 us  [routed_pairs(): lax.all_to_all(leaving, 'ep', split_axis=0, concat_axis=0, axis_index_gro...]
    all_to_all x1 -> x2, waiting for transfers between devices: 6.35 us -> 0.01 us  [sent_home(): lax.all_to_all(summed.reshape(GROUPS, span, width), 'ep', split_axis=0, c...]
    all_to_all x1 -> x2, starting transfers between devices: 5.09 us -> 10.2 us  [sent_home(): lax.all_to_all(summed.reshape(GROUPS, span, width), 'ep', split_axis=0, c...]
    dot_general x4 -> x8, matrix products: 27.5 us -> 27.5 us  [the longest x2 11.9 us: experts_on(): jnp.dot(arrived, gate_weight[0], preferred_element_type=jnp.float32)]
  transfers between devices with their start and end apart: 9 -> 11, of which waited for: 6 -> 5; matrix products, arithmetic and copies ran while one was open for 4% -> 13% of each run, Pallas kernels for 9% -> 9%
where the time goes in v2:
time: 267 us; the launch traced here: 265 us
  waiting for transfers between devices  110 us (41%)
  blocking collectives  58.2 us (22%)
  matrix products  27.5 us (10%)
  Pallas kernels  23 us (9%)
  starting transfers between devices  19.7 us (7%)
  between operations  14.1 us (5%)
  other arithmetic  10.4 us (4%)
    reduce_scatter x2, waiting for transfers between devices, sent_home(): lax.psum_scatter(product, ('ep', 'tp'), scatter_dimension=0, axis_index_g...  91.8 us
    all_gather x1, blocking collectives, routed_pairs(): lax.all_gather(notes, 'ep')  29.9 us
    all_to_all x1, blocking collectives, routed_pairs(): lax.all_to_all(leaving, 'ep', split_axis=0, concat_axis=0, axis_index_gro...  28.3 us
    ppermute x5, waiting for transfers between devices, from_earlier(): return lax.ppermute(value, 'ep', pairs)  17.6 us
    pallas_call x1, Pallas kernels, token_mixer(): pl.pallas_call(functools.partial(mixer_kernel, heads), grid=(positions //...  15.9 us
    dot_general x2, matrix products, experts_on(): jnp.dot(arrived, gate_weight[0], preferred_element_type=jnp.float32)  11.9 us
    all_to_all x2, starting transfers between devices, sent_home(): lax.all_to_all(summed.reshape(GROUPS, span, width), 'ep', split_axis=0, c...  10.2 us
    ppermute x5, starting transfers between devices, from_earlier(): return lax.ppermute(value, 'ep', pairs)  9.17 us
  transfers between devices with their start and end apart: 11, of which 5 were waited for; matrix products, arithmetic and copies ran while one was open for 13% of the time, Pallas kernels for 9%

profile of v2, /device:TPU:24, one launch (start us, length us, event | category | flops | bytes accessed | tf_op | source)
XLA Modules:
  0.0 265.3 jit_solution(10454344603939132814)
XLA Ops:
  7.2 0.0 all-gather.5.cloned.1.call-start
  7.2 0.8 constant_dynamic-slice_fusion
  8.0 0.2 reduce_window_sum.24
  8.2 1.2 fusion.22
  9.5 1.6 convolution_convert_fusion
  11.1 28.3 %all_to_all.15 = bf16[4,32,4096]{2,1,0:T(8,128)(2,1)S(1)} all-to-all(bf16[4,32,4096]{2,1,0:T(8,128)(2,1)S(1)} %convolution_convert_fusion), channel_id=1, replica_groups={{0,8,16,24},{4,12,20,28},{1,9,17,25},{5,13,21,29},{2,10,18,26},{6,14,22..., dimensions={0} | all-to-all | bytes 2097152 | tf_op jit(solution)/shard_map/all_to_all | solution.py:260
  39.3 1.1 fusion.53
  40.4 0.0 all-gather.7.cloned.1.call-start
  40.5 0.7 all-gather.7.cloned.1.call-update
  41.2 0.0 reduce-scatter.3.cloned.1.call-start
  41.2 7.0 %summary.1 = (f32[4,256,128]{2,1,0:T(8,128)}, f32[1,512]{1,0:T(1,128)}) custom-call(bf16[1024,512]{1,0:T(8,128)(2,1)} %key_ref.3, bf16[1024,1024]{1,0:T(8,128)(2,1)} %value_ref.3, f32[1024,512]{1,0:T(8,128)} %logit_ref.3), custom_call_target="tpu_custom_call" | custom-call | flops 4000000000 | bytes 5242880 | tf_op jit(solution)/shard_map/summary/pallas_call | solution.py:164
  48.3 0.7 convert_element_type.83
  49.0 3.4 %collective-permute-start.2 = (bf16[4,128]{1,0:T(4,128)(2,1)S(1)}, bf16[4,128]{1,0:T(4,128)(2,1)S(1)}, u32[]{:S(2)}, u32[]{:S(2)}) collective-permute-start(bf16[4,128]{1,0:T(4,128)(2,1)S(1)} %convert_element_type.83), channel_id=1, source_target_pairs={{0,4},{4,8},{8,12},{12,16},{16,20},{20,24},{24,28},{1,5},{5,9},{9,... | collective-permute-start | bytes 3080 | tf_op jit(solution)/shard_map/ppermute | solution.py:124
  52.3 1.1 convert_element_type.79
  53.4 1.9 collective-permute-start
  55.4 29.9 %all-gather.1 = f32[8,4,256]{2,1,0:T(4,128)S(1)} all-gather(f32[1,4,256]{2,1,0:T(4,128)S(1)} %maximum_bitcast_fusion), channel_id=2, replica_groups=mesh['ep'=8,'tp'=4] {'ep'}, dimensions={0}, use_global_device_ids=true | all-gather | bytes 36864 | tf_op jit(solution)/shard_map/all_gather | solution.py:236
  85.3 0.1 reshape.124
  85.5 1.9 reduce_window_sum.26
  87.4 0.7 multiply_convert_fusion.3
  88.1 1.3 collective-permute-start.4
  89.4 1.1 fusion.29
  90.5 1.3 collective-permute-start.1
  91.9 1.7 collective-permute-done.4
  93.6 7.0 %collective-permute-done.1 = bf16[4,256,128]{2,1,0:T(8,128)(2,1)S(1)} collective-permute-done((bf16[4,256,128]{2,1,0:T(8,128)(2,1)S(1)}, bf16[4,256,128]{2,1,0:T(8,128)(2,1)S(1)}, u32[]{:S(2)}, u32[]{:S(2)}) %collective-permute-start.1) | collective-permute-done | bytes 262176 | tf_op jit(solution)/shard_map/ppermute | solution.py:124
  100.6 1.2 add_convert_fusion
  101.8 1.3 collective-permute-start.3
  103.1 0.2 select_reduce_fusion
  103.3 0.1 reshape.125
  103.4 0.1 slice_reduce_fusion.1
  103.5 0.1 mul.131
  103.6 8.9 %collective-permute-done.3 = bf16[4,256,128]{2,1,0:T(8,128)(2,1)S(1)} collective-permute-done((bf16[4,256,128]{2,1,0:T(8,128)(2,1)S(1)}, bf16[4,256,128]{2,1,0:T(8,128)(2,1)S(1)}, u32[]{:S(2)}, u32[]{:S(2)}) %collective-permute-start.3) | collective-permute-done | bytes 262176 | tf_op jit(solution)/shard_map/ppermute | solution.py:124
  112.5 0.9 multiply_add_fusion.start_ref
  113.4 6.0 %fusion.8 = f32[512,512]{1,0:T(8,128)S(1)} fusion(bf16[512,4096]{1,0:T(8,128)(2,1)} %all-gather.5.cloned.1.call-done, bf16[1,4096,512]{2,1,0:T(8,128)(2,1)} %param.22), kind=kOutput, calls=%fused_computation.12 | convolution fusion | flops 2147483648 | bytes 9437184 | tf_op jit(solution)/shard_map/dot_general | solution.py:276
  119.5 0.0 copy-done.8
  119.5 2.4 fusion.19
  122.0 4.3 %multiply_convert_fusion.1 = bf16[512,4096]{1,0:T(8,128)(2,1)} fusion(bf16[512,512]{1,0:T(8,128)(2,1)S(1)} %fusion.19, bf16[1,512,4096]{2,1,0:T(8,128)(2,1)S(1)} %copy-done.5, f32[512]{0:T(512)S(1)} %mul.131), kind=kOutput, calls=%fused_computation.1 | convolution fusion | flops 2151677952 | bytes 8914944 | tf_op jit(solution)/shard_map/dot_general | solution.py:279
  126.3 0.2 reduce-scatter.5.cloned.1.call-start
  126.6 0.1 mul.136
  126.7 5.9 %fusion.6 = f32[512,512]{1,0:T(8,128)S(1)} fusion(bf16[512,4096]{1,0:T(8,128)(2,1)} %all-gather.7.cloned.1.call-done, bf16[1,4096,512]{2,1,0:T(8,128)(2,1)} %param.22), kind=kOutput, calls=%fused_computation.10 | convolution fusion | flops 2147483648 | bytes 9437184 | tf_op jit(solution)/shard_map/dot_general | solution.py:276
  132.6 2.4 fusion.16
  135.1 4.3 %multiply_convert_fusion = bf16[512,4096]{1,0:T(8,128)(2,1)} fusion(bf16[512,512]{1,0:T(8,128)(2,1)S(1)} %fusion.16, bf16[1,512,4096]{2,1,0:T(8,128)(2,1)S(1)} %copy-done.6, f32[512]{0:T(512)S(1)} %mul.136), kind=kOutput, calls=%fused_computation | convolution fusion | flops 2151677952 | bytes 8914944 | tf_op jit(solution)/shard_map/dot_general | solution.py:279
  139.4 42.5 %reduce-scatter.3.cloned.1.call-done = bf16[64,4096]{1,0:T(8,128)(2,1)} async-done(((bf16[512,4096]{1,0:T(8,128)(2,1)}), bf16[64,4096]{1,0:T(8,128)(2,1)}) %reduce-scatter.3.cloned.1.call-update) | async-done | bytes 524304 | tf_op jit(solution)/shard_map/reduce_scatter | solution.py:283
  181.9 5.1 %all-to-all-start.1 = ((bf16[4,16,4096]{2,1,0:T(8,128)(2,1)}), bf16[4,16,4096]{2,1,0:T(8,128)(2,1)S(1)}, u32[]{:S(2)}, u32[]{:S(2)}) async-start(bf16[4,16,4096]{2,1,0:T(8,128)(2,1)} %bitcast.61), calls=%async_computation.2 | async-start | bytes 1048576 | tf_op jit(solution)/shard_map/all_to_all | solution.py:290
  187.0 49.3 %reduce-scatter.5.cloned.1.call-done = bf16[64,4096]{1,0:T(8,128)(2,1)} async-done(((bf16[512,4096]{1,0:T(8,128)(2,1)}), bf16[64,4096]{1,0:T(8,128)(2,1)}) %reduce-scatter.5.cloned.1.call-update) | async-done | bytes 524304 | tf_op jit(solution)/shard_map/reduce_scatter | solution.py:283
  236.3 5.1 %all-to-all-start.2 = ((bf16[4,16,4096]{2,1,0:T(8,128)(2,1)}), bf16[4,16,4096]{2,1,0:T(8,128)(2,1)S(1)}, u32[]{:S(2)}, u32[]{:S(2)}) async-start(bf16[4,16,4096]{2,1,0:T(8,128)(2,1)} %bitcast.62), calls=%async_computation.4 | async-start | bytes 1048576 | tf_op jit(solution)/shard_map/all_to_all | solution.py:290
  241.4 15.9 %mixer.1 = bf16[1024,1024]{1,0:T(8,128)(2,1)} custom-call(bf16[1024,512]{1,0:T(8,128)(2,1)} %query_ref.1, bf16[1024,512]{1,0:T(8,128)(2,1)} %key_ref.3, bf16[1024,1024]{1,0:T(8,128)(2,1)} %value_ref.3, f32[1024,512]{1,0:T(8,128)} %logit_ref.3, f32[4,256,128]{2,1,0:T(8,128)} %multiply_add_fusion.start_ref, f32[1,256]{1,0:T(1,128)} %bitcast.70), custom_call_target="tpu_custom_call" | custom-call | flops 16000000000 | bytes 8388608 | tf_op jit(solution)/shard_map/mixer/pallas_call | solution.py:185
  257.4 0.5 multiply_reduce_fusion
  257.8 1.0 multiply_convert_fusion.2
  (38 shorter events, 0.3 us)
Async XLA Ops:
  7.2 106.3 %all-gather.5.cloned.1.call-start = ((), (), s32[]{:S(2)}) async-start(), calls=%async_computation.5 | async-start | bytes 4718592 | tf_op jit(solution)/shard_map/all_gather | solution.py:268
  40.4 86.2 %all-gather.7.cloned.1.call-start = ((), (), s32[]{:S(2)}) async-start(), calls=%async_computation.7 | async-start | bytes 4718592 | tf_op jit(solution)/shard_map/all_gather | solution.py:268
  41.2 14.2 %copy-start.1 = (s32[256,2]{0,1:T(2,128)S(1)}, s32[256,2]{0,1:T(2,128)}, u32[]{:S(2)}) copy-start(s32[256,2]{0,1:T(2,128)} %param.20) | copy-start | bytes 6148
  41.2 14.2 %copy-start.2 = (f32[256,2]{0,1:T(2,128)S(1)}, f32[256,2]{0,1:T(2,128)}, u32[]{:S(2)}) copy-start(f32[256,2]{0,1:T(2,128)} %param.21) | copy-start | bytes 6148
  41.2 140.7 %reduce-scatter.3.cloned.1.call-start = ((), (), s32[]{:S(2)}) async-start(), calls=%async_computation.6 | async-start | bytes 4718592 | tf_op jit(solution)/shard_map/reduce_scatter | solution.py:283
  49.0 38.5 %collective-permute-start.2 = (bf16[4,128]{1,0:T(4,128)(2,1)S(1)}, bf16[4,128]{1,0:T(4,128)(2,1)S(1)}, u32[]{:S(2)}, u32[]{:S(2)}) collective-permute-start(bf16[4,128]{1,0:T(4,128)(2,1)S(1)} %convert_element_type.83), channel_id=1, source_target_pairs={{0,4},{4,8},{8,12},{12,16},{16,20},{20,24},{24,28},{1,5},{5,9},{9,... | collective-permute-start | bytes 3080 | tf_op jit(solution)/shard_map/ppermute | solution.py:124
  53.4 36.0 %collective-permute-start = (bf16[4,256,128]{2,1,0:T(8,128)(2,1)S(1)}, bf16[4,256,128]{2,1,0:T(8,128)(2,1)S(1)}, u32[]{:S(2)}, u32[]{:S(2)}) collective-permute-start(bf16[4,256,128]{2,1,0:T(8,128)(2,1)S(1)} %convert_element_type.79), channel_id=1, source_target_pairs={{0,4},{4,8},{8,12},{12,16},{16,20},{20,24},{24,28},{1,5},{5,9},{9,... | collective-permute-start | bytes 786440 | tf_op jit(solution)/shard_map/ppermute | solution.py:124
  88.1 5.5 %collective-permute-start.4 = (bf16[4,128]{1,0:T(4,128)(2,1)S(1)}, bf16[4,128]{1,0:T(4,128)(2,1)S(1)}, u32[]{:S(2)}, u32[]{:S(2)}) collective-permute-start(bf16[4,128]{1,0:T(4,128)(2,1)S(1)} %multiply_convert_fusion.3), channel_id=1, source_target_pairs={{0,8},{4,12},{8,16},{12,20},{16,24},{20,28},{1,9},{5,13},{9,17},{1... | collective-permute-start | bytes 3080 | tf_op jit(solution)/shard_map/ppermute | solution.py:124
  90.5 10.0 %collective-permute-start.1 = (bf16[4,256,128]{2,1,0:T(8,128)(2,1)S(1)}, bf16[4,256,128]{2,1,0:T(8,128)(2,1)S(1)}, u32[]{:S(2)}, u32[]{:S(2)}) collective-permute-start(bf16[4,256,128]{2,1,0:T(8,128)(2,1)S(1)} %fusion.29), channel_id=1, source_target_pairs={{0,8},{4,12},{8,16},{12,20},{16,24},{20,28},{1,9},{5,13},{9,17},{1... | collective-permute-start | bytes 786440 | tf_op jit(solution)/shard_map/ppermute | solution.py:124
  101.8 10.8 %collective-permute-start.3 = (bf16[4,256,128]{2,1,0:T(8,128)(2,1)S(1)}, bf16[4,256,128]{2,1,0:T(8,128)(2,1)S(1)}, u32[]{:S(2)}, u32[]{:S(2)}) collective-permute-start(bf16[4,256,128]{2,1,0:T(8,128)(2,1)S(1)} %add_convert_fusion), channel_id=1, source_target_pairs={{0,16},{4,20},{8,24},{12,28},{1,17},{5,21},{9,25},{13,29},{2,18},{... | collective-permute-start | bytes 786440 | tf_op jit(solution)/shard_map/ppermute | solution.py:124
  113.4 6.0 %copy-start.3 = (bf16[1,4096,512]{2,1,0:T(8,128)(2,1)S(1)}, bf16[1,4096,512]{2,1,0:T(8,128)(2,1)}, u32[]{:S(2)}) copy-start(bf16[1,4096,512]{2,1,0:T(8,128)(2,1)} %param.23) | copy-start | bytes 12582916
  113.4 6.1 %copy-start.8 = (bf16[512,4096]{1,0:T(8,128)(2,1)S(1)}, bf16[512,4096]{1,0:T(8,128)(2,1)}, u32[]{:S(2)}) copy-start(bf16[512,4096]{1,0:T(8,128)(2,1)} %all-gather.5.cloned.1.call-done) | copy-start | bytes 12582916
  119.5 2.5 copy-start.5
  126.3 110.0 %reduce-scatter.5.cloned.1.call-start = ((), (), s32[]{:S(2)}) async-start(), calls=%async_computation.8 | async-start | bytes 4718592 | tf_op jit(solution)/shard_map/reduce_scatter | solution.py:283
  126.7 5.9 %copy-start.4 = (bf16[1,4096,512]{2,1,0:T(8,128)(2,1)S(1)}, bf16[1,4096,512]{2,1,0:T(8,128)(2,1)}, u32[]{:S(2)}) copy-start(bf16[1,4096,512]{2,1,0:T(8,128)(2,1)} %param.23) | copy-start | bytes 12582916
  126.7 5.9 %copy-start.7 = (bf16[512,4096]{1,0:T(8,128)(2,1)S(1)}, bf16[512,4096]{1,0:T(8,128)(2,1)}, u32[]{:S(2)}) copy-start(bf16[512,4096]{1,0:T(8,128)(2,1)} %all-gather.7.cloned.1.call-done) | copy-start | bytes 12582916
  132.6 2.5 copy-start.6
  181.9 54.4 %all-to-all-start.1 = ((bf16[4,16,4096]{2,1,0:T(8,128)(2,1)}), bf16[4,16,4096]{2,1,0:T(8,128)(2,1)S(1)}, u32[]{:S(2)}, u32[]{:S(2)}) async-start(bf16[4,16,4096]{2,1,0:T(8,128)(2,1)} %bitcast.61), calls=%async_computation.2 | async-start | bytes 1048576 | tf_op jit(solution)/shard_map/all_to_all | solution.py:290
  236.3 21.0 %all-to-all-start.2 = ((bf16[4,16,4096]{2,1,0:T(8,128)(2,1)}), bf16[4,16,4096]{2,1,0:T(8,128)(2,1)S(1)}, u32[]{:S(2)}, u32[]{:S(2)}) async-start(bf16[4,16,4096]{2,1,0:T(8,128)(2,1)} %bitcast.62), calls=%async_computation.4 | async-start | bytes 1048576 | tf_op jit(solution)/shard_map/all_to_all | solution.py:290
  241.4 16.4 %copy-start = (f32[4096]{0:T(1024)S(1)}, f32[4096]{0:T(1024)}, u32[]{:S(2)}) copy-start(f32[4096]{0:T(1024)} %param.25) | copy-start | bytes 49156
Sparse Core Ops, SparseCore 0:
  40.5 41.3 all-gather.4
  84.4 36.6 all-gather.6
  126.5 55.4 reduce-scatter.2
  185.2 51.1 reduce-scatter.4
